TPU v7x, 32 devices: a whole 2x2x4 slice. The times are simulated.
32 devices in a mesh: ep: 16 (over z, y, x), tp: 2 (over core).
Axes of the slice: x: 2, y: 2, z: 4, core: 2. Of those that a mesh axis runs over, the one named last changes fastest.
Arguments:
- tokens: bfloat16 [256, 2048], P('ep'), may hold values from -6 to 6
- lengths: int32 [256], P('ep'), may hold values from 1024 to 8191
- prior_state: float32 [256, 16, 64, 64], P('ep', 'tp'), may hold values from -2 to 2
- mix_gain: float32 [2048], replicated, may hold values from 0.1 to 1.9
- post_gain: float32 [2048], replicated, may hold values from 0.1 to 1.9
- ffn_gain: float32 [2048], replicated, may hold values from 0.1 to 1.9
- out_gain: float32 [2048], replicated, may hold values from 0.1 to 1.9
- query_weight: bfloat16 [2048, 1024], P('ep', 'tp'), may hold values from -0.125 to 0.125
- key_weight: bfloat16 [2048, 1024], P('ep', 'tp'), may hold values from -0.125 to 0.125
- value_weight: bfloat16 [2048, 1024], P('ep', 'tp'), may hold values from -0.125 to 0.125
- gate_weight: bfloat16 [2048, 1024], P('ep', 'tp'), may hold values from -0.125 to 0.125
- out_weight: bfloat16 [1024, 2048], P('tp', 'ep'), may hold values from -0.1875 to 0.1875
- routes: int32 [256, 6], P('ep'), may hold values from 0 to 15, all different within a row; in each aligned block of 16 rows (0 to 15, 16 to 31, ...) at most 8 rows name the same one
- route_gates: float32 [256, 6], P('ep'), may hold values from 0.1 to 0.9
- expert_gate: bfloat16 [16, 2048, 512], P('ep', None, 'tp'), may hold values from -0.125 to 0.125
- expert_up: bfloat16 [16, 2048, 512], P('ep', None, 'tp'), may hold values from -0.125 to 0.125
- expert_down: bfloat16 [16, 512, 2048], P('ep', 'tp'), may hold values from -0.25 to 0.25
- shared_gate: bfloat16 [2048, 512], P(None, 'tp'), may hold values from -0.125 to 0.125
- shared_up: bfloat16 [2048, 512], P(None, 'tp'), may hold values from -0.125 to 0.125
- shared_down: bfloat16 [512, 2048], P('tp'), may hold values from -0.25 to 0.25
Outputs:
- result: bfloat16 [256, 2048], P('ep')
- new_state: float32 [256, 16, 64, 64], P('ep', 'tp')
Inputs may be any that keep to these rules, and one draw needn't show every extreme that they name: `routes`: each row names 6 different experts. In the rows of one device (aligned blocks of 16 rows) no expert is named more than 8 times, and in every draw some expert is named exactly 8 times in some block.
All inputs are finite; a program needn't handle non-finite values.
Results may differ from a plain program's by a relative error of at most 0.02.
Values may be sent and summed in bfloat16 or wider, within the bound.
A program may use at most 128 MiB of HBM per device.

v0:
```python
import jax
import jax.numpy as jnp
from jax import lax
from jax.sharding import PartitionSpec as P

HEAD = 64
HEADS = 16
EPS = 1e-06
THETA = 10000.0


def rounded(values):
    return lax.optimization_barrier(values.astype(jnp.bfloat16)).astype(jnp.float32)


def scaled_rows(values, gain_row):
    widened = values.astype(jnp.float32)
    return widened * lax.rsqrt(jnp.mean(widened * widened, axis=-1, keepdims=True) + EPS) * gain_row


def rotate(vectors, lengths):
    half_dim = vectors.shape[-1] // 2
    frequency = THETA ** (-jnp.arange(half_dim, dtype=jnp.float32) / half_dim)
    angles = lengths.astype(jnp.float32)[:, None] * frequency[None, :]
    cosine = jnp.cos(angles)[:, None, :]
    sine_part = jnp.sin(angles)[:, None, :]
    leading = vectors[..., :half_dim]
    trailing = vectors[..., half_dim:]
    return jnp.concatenate(
        [leading * cosine - trailing * sine_part, trailing * cosine + leading * sine_part], axis=-1
    )


def decay_table(head_count):
    head_order = jnp.arange(head_count, dtype=jnp.float32)
    return 1.0 - jnp.exp2(-5.0 - 7.0 * head_order / (head_count - 1))


def retain(queries, keys_new, values, out_gate, prior_state, lengths, decays):
    seq_count = queries.shape[0]
    head_count = decays.shape[0]
    layout = (seq_count, head_count, HEAD)
    rot_query = rotate(queries.astype(jnp.float32).reshape(layout), lengths)
    rot_key = rotate(keys_new.astype(jnp.float32).reshape(layout), lengths) * HEAD ** (-0.5)
    wide_values = values.astype(jnp.float32).reshape(layout)
    from_state = jnp.einsum(
        "shd,shde->she", rot_query, prior_state, precision=lax.Precision.HIGHEST
    )
    self_term = jnp.sum(rot_query * rot_key, axis=-1, keepdims=True)
    read_out = decays[None, :, None] * from_state + self_term * wide_values
    new_state = (
        decays[None, :, None, None] * prior_state
        + rot_key[..., :, None] * wide_values[..., None, :]
    )
    normed = read_out * lax.rsqrt(jnp.mean(read_out * read_out, axis=-1, keepdims=True) + EPS)
    gated_rows = normed.reshape(seq_count, head_count * HEAD) * jax.nn.silu(
        out_gate.astype(jnp.float32)
    )
    return (gated_rows.astype(jnp.bfloat16), new_state)


def on_device(
    tokens,
    lengths,
    prior_state,
    mix_gain,
    post_gain,
    ffn_gain,
    out_gain,
    query_weight,
    key_weight,
    value_weight,
    gate_weight,
    out_weight,
    routes,
    route_gates,
    expert_gate,
    expert_up,
    expert_down,
    shared_gate,
    shared_up,
    shared_down,
):
    seq_here = tokens.shape[0]
    model_width = tokens.shape[1]
    local_cols = query_weight.shape[1]
    normed = scaled_rows(tokens, mix_gain).astype(jnp.bfloat16)
    features = lax.all_to_all(normed, "ep", split_axis=1, concat_axis=0, tiled=True)
    joined = jnp.concatenate((query_weight, key_weight, value_weight, gate_weight), axis=1)
    summed = lax.psum_scatter(
        jnp.dot(features, joined, preferred_element_type=jnp.float32),
        "ep",
        scatter_dimension=0,
        tiled=True,
    )
    projected = tuple((summed[:, role * local_cols : (role + 1) * local_cols] for role in range(4)))
    queries, keys_new, values, out_gate = tuple(
        (member.astype(jnp.bfloat16) for member in projected)
    )
    heads_here = local_cols // HEAD
    decays = lax.dynamic_slice_in_dim(
        decay_table(HEADS), lax.axis_index("tp") * heads_here, heads_here, 0
    )
    retained, new_state = retain(queries, keys_new, values, out_gate, prior_state, lengths, decays)
    column_part = jnp.dot(
        lax.all_gather(retained, "ep", axis=0, tiled=True),
        out_weight,
        preferred_element_type=jnp.float32,
    ).astype(jnp.bfloat16)
    partial_mix = lax.all_to_all(column_part, "ep", split_axis=0, concat_axis=1, tiled=True).astype(
        jnp.float32
    )
    mixed_sum = rounded(
        lax.psum(rounded(partial_mix).astype(jnp.bfloat16), "tp").astype(jnp.float32)
    )
    middle = rounded(tokens.astype(jnp.float32) + scaled_rows(mixed_sum, post_gain))
    moe_in = scaled_rows(middle, ffn_gain).astype(jnp.bfloat16)
    experts_all = lax.axis_size("ep")
    topk_here = routes.shape[1]
    capacity = seq_here * topk_here // experts_all + 2
    slot_count = experts_all * capacity
    flat_routes = routes.reshape(-1)
    onehot = (flat_routes[:, None] == jnp.arange(experts_all, dtype=jnp.int32)[None, :]).astype(
        jnp.int32
    )
    earlier = jnp.cumsum(onehot, axis=0) - onehot
    ranks = jnp.sum(earlier * onehot, axis=1)
    slot_ids = flat_routes * capacity + ranks
    placing = (jnp.arange(slot_count, dtype=jnp.int32)[:, None] == slot_ids[None, :]).reshape(
        slot_count, seq_here, topk_here
    )
    dispatch_rows = jnp.any(placing, axis=2).astype(jnp.bfloat16)
    combine = jnp.sum(
        jnp.where(placing, route_gates[None, :, :], jnp.zeros((), jnp.float32)), axis=2
    ).T
    outgoing = jnp.dot(dispatch_rows, moe_in, preferred_element_type=jnp.float32).astype(
        jnp.bfloat16
    )
    outgoing = outgoing.reshape(experts_all, capacity, model_width)
    gate_local = expert_gate[0]
    up_local = expert_up[0]
    down_local = expert_down[0]
    arrived = lax.all_to_all(outgoing, "ep", split_axis=0, concat_axis=0, tiled=True)
    sources = arrived.shape[0]
    held_slots = arrived.shape[1]
    flat_in = arrived.reshape(sources * held_slots, model_width)
    hidden = (
        jax.nn.silu(jnp.dot(flat_in, gate_local, preferred_element_type=jnp.float32))
        * jnp.dot(flat_in, up_local, preferred_element_type=jnp.float32)
    ).astype(jnp.bfloat16)
    partial_out = rounded(jnp.dot(hidden, down_local, preferred_element_type=jnp.float32))
    expert_sum = lax.psum(partial_out.astype(jnp.bfloat16), "tp")
    returned = lax.all_to_all(
        expert_sum.reshape(sources, held_slots, -1), "ep", split_axis=0, concat_axis=0, tiled=True
    )
    back_rows = returned.reshape(slot_count, -1).astype(jnp.float32)
    routed = jnp.dot(combine, back_rows, precision=lax.Precision.HIGHEST)
    shared_hidden = (
        jax.nn.silu(jnp.dot(moe_in, shared_gate, preferred_element_type=jnp.float32))
        * jnp.dot(moe_in, shared_up, preferred_element_type=jnp.float32)
    ).astype(jnp.bfloat16)
    shared_part = rounded(jnp.dot(shared_hidden, shared_down, preferred_element_type=jnp.float32))
    shared_out = lax.psum(shared_part.astype(jnp.bfloat16), "tp")
    mixture = shared_out.astype(jnp.float32) + routed
    result = (middle + scaled_rows(mixture, out_gain)).astype(jnp.bfloat16)
    return (result, new_state)


def solution(mesh):
    return jax.shard_map(
        on_device,
        mesh=mesh,
        in_specs=(
            P("ep", None),
            P("ep"),
            P("ep", "tp", None, None),
            P(),
            P(),
            P(),
            P(),
            P("ep", "tp"),
            P("ep", "tp"),
            P("ep", "tp"),
            P("ep", "tp"),
            P("tp", "ep"),
            P("ep", None),
            P("ep", None),
            P("ep", None, "tp"),
            P("ep", None, "tp"),
            P("ep", "tp", None),
            P(None, "tp"),
            P(None, "tp"),
            P("tp", None),
        ),
        out_specs=(P("ep", None), P("ep", "tp", None, None)),
        check_vma=False,
    )
```

profile of v0, /device:TPU:0, one launch (start us, length us, event | category | flops | bytes accessed | tf_op | source)
XLA Modules:
  0.0 254.3 jit_solution(6704595756294250518)
XLA Ops:
  7.2 1.0 fusion.25
  8.3 0.9 copy_bitcast_fusion.1
  9.2 15.7 %all_to_all.48 = bf16[16,16,128]{2,0,1:T(8,128)(2,1)S(1)} all-to-all(bf16[16,16,128]{2,0,1:T(8,128)(2,1)S(1)} %copy_bitcast_fusion.1), channel_id=1, replica_groups=mesh['ep'=16,'tp'=2] {'ep'}, dimensions={1} | all-to-all | bytes 131072 | tf_op jit(solution)/shard_map/all_to_all | solution.py:88
  24.9 2.8 %fusion.11 = f32[256,2048]{1,0:T(8,128)} fusion(bf16[256,128]{1,0:T(8,128)(2,1)S(1)} %bitcast.57, bf16[128,512]{1,0:T(8,128)(2,1)} %param.30, bf16[128,512]{1,0:T(8,128)(2,1)} %param.29, bf16[128,512]{1,0:T(8,128)(2,1)} %param.28, bf16[128,512]{1,0:T(8,128)(2,1)} %param.27), kind=kOutput, calls=%fused_computation.18 | convolution fusion | flops 136314880 | bytes 2686976 | tf_op jit(solution)/shard_map/dot_general | solution.py:91
  28.8 77.1 %reduce-scatter.2.cloned.1.call-done = f32[16,2048]{1,0:T(8,128)} async-done(((f32[256,2048]{1,0:T(8,128)}), f32[16,2048]{1,0:T(8,128)}) %reduce-scatter.2.cloned.1.call-update) | async-done | bytes 131088 | tf_op jit(solution)/shard_map/reduce_scatter | solution.py:90
  105.9 0.9 convert.9
  107.3 5.3 %fusion.62 = f32[16,8,1,64]{3,2,1,0:T(1,128)S(1)} fusion(f32[16,8,64,1]{2,3,1,0:T(1,128)S(1)} %bitcast.55, f32[16,8,64,64]{3,2,1,0:T(8,128)} %param.22), kind=kOutput, calls=%fused_computation.103 | convolution fusion | flops 6291456 | bytes 2162688 | tf_op jit(solution)/shard_map/shd,shde->she/dot_general | solution.py:46
  113.0 38.2 %all_gather.3 = bf16[256,512]{1,0:T(8,128)(2,1)S(1)} all-gather(bf16[16,512]{1,0:T(8,128)(2,1)S(1)} %fusion.46), channel_id=1, replica_groups=mesh['ep'=16,'tp'=2] {'ep'}, dimensions={0}, use_global_device_ids=true | all-gather | bytes 278528 | tf_op jit(solution)/shard_map/all_gather | solution.py:106
  152.1 3.5 %all-to-all-start.1 = ((bf16[16,16,128]{2,1,0:T(8,128)(2,1)}), bf16[16,16,128]{2,1,0:T(8,128)(2,1)S(1)}, u32[]{:S(2)}, u32[]{:S(2)}) async-start(bf16[16,16,128]{2,1,0:T(8,128)(2,1)} %bitcast.6), calls=%async_computation.2 | async-start | bytes 131072 | tf_op jit(solution)/shard_map/all_to_all | solution.py:110
  155.6 7.4 %all-to-all-done.1 = bf16[16,16,128]{2,1,0:T(8,128)(2,1)S(1)} async-done(((bf16[16,16,128]{2,1,0:T(8,128)(2,1)}), bf16[16,16,128]{2,1,0:T(8,128)(2,1)S(1)}, u32[]{:S(2)}, u32[]{:S(2)}) %all-to-all-start.1) | async-done | bytes 65568 | tf_op jit(solution)/shard_map/all_to_all | solution.py:110
  163.8 14.5 %all-reduce.4.cloned.1.call-done = bf16[16,2048]{1,0:T(8,128)(2,1)} async-done(((bf16[16,2048]{1,0:T(8,128)(2,1)}), bf16[16,2048]{1,0:T(8,128)(2,1)}) %all-reduce.4.cloned.1.call-update) | async-done | bytes 65552 | tf_op jit(solution)/shard_map/psum | solution.py:114
  178.3 1.0 fusion.23
  179.3 0.9 fusion.28
  180.4 1.1 fusion.1
  181.5 6.8 %all-to-all-start.2 = ((bf16[16,8,2048]{2,1,0:T(8,128)(2,1)}), bf16[16,8,2048]{2,1,0:T(8,128)(2,1)S(1)}, u32[]{:S(2)}, u32[]{:S(2)}) async-start(bf16[16,8,2048]{2,1,0:T(8,128)(2,1)} %fusion.1), calls=%async_computation.3 | async-start | bytes 1048576 | tf_op jit(solution)/shard_map/all_to_all | solution.py:143
  188.4 1.5 fusion.60
  189.9 3.0 %convolution_convert_fusion.2 = bf16[16,2048]{1,0:T(8,128)(2,1)} fusion(bf16[256,2048]{1,0:T(8,128)(2,1)} %param.39, bf16[2048,256]{1,0:T(8,128)(2,1)} %param.38, f32[16,256]{1,0:T(8,128)S(1)} %fusion.60, bf16[16,2048]{1,0:T(8,128)(2,1)S(1)} %fusion.28, f32[2048]{0:T(1024)S(1)} %copy-done.4, f32[16]{0:T(128)S(1)} %add_rsqrt_fusion.2), kind=kOutput, calls=%fused_computation.6 | convolution fusion | flops 33742848 | bytes 2252864 | tf_op jit(solution)/shard_map/dot_general | solution.py:162
  192.9 10.9 %all-to-all-done.2 = bf16[16,8,2048]{2,1,0:T(8,128)(2,1)S(1)} async-done(((bf16[16,8,2048]{2,1,0:T(8,128)(2,1)}), bf16[16,8,2048]{2,1,0:T(8,128)(2,1)S(1)}, u32[]{:S(2)}, u32[]{:S(2)}) %all-to-all-start.2) | async-done | bytes 524320 | tf_op jit(solution)/shard_map/all_to_all | solution.py:143
  203.8 1.5 fusion.9
  205.4 1.6 convolution_convert_fusion
  207.0 17.3 %all-reduce.6.cloned.1.call-done = (bf16[16,8,2048]{2,1,0:T(8,128)(2,1)}, bf16[16,2048]{1,0:T(8,128)(2,1)}) async-done(((bf16[16,8,2048]{2,1,0:T(8,128)(2,1)}, bf16[16,2048]{1,0:T(8,128)(2,1)}), (bf16[16,8,2048]{2,1,0:T(8,128)(2,1)}, bf16[16,2048]{1,0:T(8,128)(2,1)})) %all-reduce.6.cloned.1.call-update) | async-done | bytes 589840 | tf_op jit(solution)/shard_map/psum | solution.py:152
  224.3 6.8 %all-to-all-start.3 = ((bf16[16,8,2048]{2,1,0:T(8,128)(2,1)}), bf16[16,8,2048]{2,1,0:T(8,128)(2,1)S(1)}, u32[]{:S(2)}, u32[]{:S(2)}) async-start(bf16[16,8,2048]{2,1,0:T(8,128)(2,1)} %get-tuple-element.2), calls=%async_computation.4 | async-start | bytes 1048576 | tf_op jit(solution)/shard_map/all_to_all | solution.py:153
  231.2 4.3 %multiply_add_fusion = f32[16,8,64,64]{3,2,1,0:T(8,128)} fusion(f32[16,8,64,64]{3,2,1,0:T(8,128)} %param.22, f32[16,8,64]{2,1,0:T(8,128)S(1)} %reshape.193, f32[16,8,64]{2,1,0:T(8,128)S(1)} %get-tuple-element.20, f32[8]{0:T(128)S(1)} %dynamic_slice.3), kind=kLoop, calls=%fused_computation.1 | loop fusion | flops 1572864 | bytes 4259872 | tf_op jit(solution)/shard_map/add | solution.py:52
  235.5 11.1 %all-to-all-done.3 = bf16[16,8,2048]{2,1,0:T(8,128)(2,1)S(1)} async-done(((bf16[16,8,2048]{2,1,0:T(8,128)(2,1)}), bf16[16,8,2048]{2,1,0:T(8,128)(2,1)S(1)}, u32[]{:S(2)}, u32[]{:S(2)}) %all-to-all-start.3) | async-done | bytes 524320 | tf_op jit(solution)/shard_map/all_to_all | solution.py:153
  (63 shorter events, 5.0 us)
Async XLA Ops:
  7.2 198.2 %copy-start = (bf16[1,256,2048]{2,1,0:T(8,128)(2,1)S(1)}, bf16[1,256,2048]{2,1,0:T(8,128)(2,1)}, u32[]{:S(2)}) copy-start(bf16[1,256,2048]{2,1,0:T(8,128)(2,1)} %param.36) | copy-start | bytes 3145732
  7.2 20.6 %copy-start.10 = (s32[16]{0:T(128)S(1)}, s32[16]{0:T(128)}, u32[]{:S(2)}) copy-start(s32[16]{0:T(128)} %param.21) | copy-start | bytes 196
  7.2 20.6 %copy-start.6 = (s32[16,6]{0,1:T(8,128)S(1)}, s32[16,6]{0,1:T(8,128)}, u32[]{:S(2)}) copy-start(s32[16,6]{0,1:T(8,128)} %param.32) | copy-start | bytes 1156
  7.2 98.7 %reduce-scatter.2.cloned.1.call-start = ((), (), s32[]{:S(2)}) async-start(), calls=%async_computation.5 | async-start | bytes 2228224 | tf_op jit(solution)/shard_map/reduce_scatter | solution.py:90
  27.7 123.5 %copy-start.3 = (bf16[512,128]{1,0:T(8,128)(2,1)S(1)}, bf16[512,128]{1,0:T(8,128)(2,1)}, u32[]{:S(2)}) copy-start(bf16[512,128]{1,0:T(8,128)(2,1)} %param.31) | copy-start | bytes 393220
  27.8 151.5 %copy-start.2 = (bf16[16,2048]{1,0:T(8,128)(2,1)S(1)}, bf16[16,2048]{1,0:T(8,128)(2,1)}, u32[]{:S(2)}) copy-start(bf16[16,2048]{1,0:T(8,128)(2,1)} %param.20) | copy-start | bytes 196612
  27.8 151.5 %copy-start.7 = (f32[2048]{0:T(1024)S(1)}, f32[2048]{0:T(1024)}, u32[]{:S(2)}) copy-start(f32[2048]{0:T(1024)} %param.24) | copy-start | bytes 24580
  27.8 152.6 %copy-start.4 = (f32[2048]{0:T(1024)S(1)}, f32[2048]{0:T(1024)}, u32[]{:S(2)}) copy-start(f32[2048]{0:T(1024)} %param.25) | copy-start | bytes 24580
  112.9 92.5 %copy-start.1 = (bf16[1,2048,256]{2,1,0:T(8,128)(2,1)S(1)}, bf16[1,2048,256]{2,1,0:T(8,128)(2,1)}, u32[]{:S(2)}) copy-start(bf16[1,2048,256]{2,1,0:T(8,128)(2,1)} %param.35) | copy-start | bytes 3145732
  152.1 11.0 %all-to-all-start.1 = ((bf16[16,16,128]{2,1,0:T(8,128)(2,1)}), bf16[16,16,128]{2,1,0:T(8,128)(2,1)S(1)}, u32[]{:S(2)}, u32[]{:S(2)}) async-start(bf16[16,16,128]{2,1,0:T(8,128)(2,1)} %bitcast.6), calls=%async_computation.2 | async-start | bytes 131072 | tf_op jit(solution)/shard_map/all_to_all | solution.py:110
  155.6 22.7 %all-reduce.4.cloned.1.call-start = ((), (), s32[]{:S(2)}) async-start(), calls=%async_computation.6 | async-start | bytes 131072 | tf_op jit(solution)/shard_map/psum | solution.py:114
  181.5 22.3 %all-to-all-start.2 = ((bf16[16,8,2048]{2,1,0:T(8,128)(2,1)}), bf16[16,8,2048]{2,1,0:T(8,128)(2,1)S(1)}, u32[]{:S(2)}, u32[]{:S(2)}) async-start(bf16[16,8,2048]{2,1,0:T(8,128)(2,1)} %fusion.1), calls=%async_computation.3 | async-start | bytes 1048576 | tf_op jit(solution)/shard_map/all_to_all | solution.py:143
  188.4 35.9 %all-reduce.6.cloned.1.call-start = ((), (), s32[]{:S(2)}) async-start(), calls=%async_computation.7 | async-start | bytes 1179648 | tf_op jit(solution)/shard_map/psum | solution.py:152
  189.9 41.2 %copy-start.9 = (f32[16,6]{0,1:T(8,128)S(1)}, f32[16,6]{0,1:T(8,128)}, u32[]{:S(2)}) copy-start(f32[16,6]{0,1:T(8,128)} %param.33) | copy-start | bytes 1156
  224.3 22.3 %all-to-all-start.3 = ((bf16[16,8,2048]{2,1,0:T(8,128)(2,1)}), bf16[16,8,2048]{2,1,0:T(8,128)(2,1)S(1)}, u32[]{:S(2)}, u32[]{:S(2)}) async-start(bf16[16,8,2048]{2,1,0:T(8,128)(2,1)} %get-tuple-element.2), calls=%async_computation.4 | async-start | bytes 1048576 | tf_op jit(solution)/shard_map/all_to_all | solution.py:153
  231.2 15.4 %copy-start.5 = (bf16[16,2048]{1,0:T(8,128)(2,1)S(1)}, bf16[16,2048]{1,0:T(8,128)(2,1)}, u32[]{:S(2)}) copy-start(bf16[16,2048]{1,0:T(8,128)(2,1)} %get-tuple-element.3) | copy-start | bytes 196612
  231.2 15.8 %copy-start.8 = (f32[2048]{0:T(1024)S(1)}, f32[2048]{0:T(1024)}, u32[]{:S(2)}) copy-start(f32[2048]{0:T(1024)} %param.26) | copy-start | bytes 24580
Sparse Core Ops, SparseCore 0:
  27.9 77.9 reduce-scatter.1
  163.9 14.3 all-reduce.3
  207.1 17.0 all-reduce.5
where the time goes:
time: 255 us; the launch traced here: 254 us
  waiting for transfers between devices  138 us (54%)
  blocking collectives  53.9 us (21%)
  matrix products  18.1 us (7%)
  starting transfers between devices  17.3 us (7%)
  between operations  14.1 us (6%)
  other arithmetic  11.2 us (4%)
    reduce_scatter x1, waiting for transfers between devices, on_device(): lax.psum_scatter(jnp.dot(features, joined, preferred_element_type=jnp.flo...  77.1 us
    all_gather x1, blocking collectives, on_device(): lax.all_gather(retained, 'ep', axis=0, tiled=True)  38.2 us
    psum x1, waiting for transfers between devices, on_device(): expert_sum = lax.psum(partial_out.astype(jnp.bfloat16), 'tp')  17.3 us
    all_to_all x1, blocking collectives, on_device(): lax.all_to_all(normed, 'ep', split_axis=1, concat_axis=0, tiled=True)  15.7 us
    psum x1, waiting for transfers between devices, on_device(): lax.psum(rounded(partial_mix).astype(jnp.bfloat16), 'tp')  14.5 us
    all_to_all x1, waiting for transfers between devices, on_device(): lax.all_to_all(expert_sum.reshape(sources, held_slots, -1), 'ep', split_a...  11.1 us
    all_to_all x1, waiting for transfers between devices, on_device(): lax.all_to_all(outgoing, 'ep', split_axis=0, concat_axis=0, tiled=True)  10.9 us
    all_to_all x1, waiting for transfers between devices, on_device(): lax.all_to_all(column_part, 'ep', split_axis=0, concat_axis=1, tiled=True)  7.44 us
  transfers between devices with their start and end apart: 6, of which 6 were waited for; matrix products, arithmetic and copies ran while one was open for 4% of the time, Pallas kernels for 0%

commit v1 on v0

--- a/solution.py
+++ b/solution.py
@@ -85,7 +85,9 @@
     model_width = tokens.shape[1]
     local_cols = query_weight.shape[1]
     normed = scaled_rows(tokens, mix_gain).astype(jnp.bfloat16)
-    features = lax.all_to_all(normed, "ep", split_axis=1, concat_axis=0, tiled=True)
+    shards = jnp.split(normed, lax.axis_size("ep"), axis=1)
+    got = lax.all_to_all(jnp.stack(shards), "ep", 0, 0)
+    features = jnp.concatenate(got, axis=0)
     joined = jnp.concatenate((query_weight, key_weight, value_weight, gate_weight), axis=1)
     summed = lax.psum_scatter(
         jnp.dot(features, joined, preferred_element_type=jnp.float32),

time: 255 us -> 255 us (level)
  no operation moved by 1% of the time
where the time goes in v1:
time: 255 us
  waiting for transfers between devices  138 us (54%)
  blocking collectives  53.9 us (21%)
  matrix products  18.1 us (7%)
  starting transfers between devices  17.3 us (7%)
  between operations  14.1 us (6%)
  other arithmetic  11.2 us (4%)
    reduce_scatter x1, waiting for transfers between devices, on_device(): lax.psum_scatter(jnp.dot(features, joined, preferred_element_type=jnp.flo...  77.1 us
    all_gather x1, blocking collectives, on_device(): lax.all_gather(retained, 'ep', axis=0, tiled=True)  38.2 us
    psum x1, waiting for transfers between devices, on_device(): expert_sum = lax.psum(partial_out.astype(jnp.bfloat16), 'tp')  17.3 us
    all_to_all x1, blocking collectives, on_device(): got = lax.all_to_all(jnp.stack(shards), 'ep', 0, 0)  15.7 us
    psum x1, waiting for transfers between devices, on_device(): lax.psum(rounded(partial_mix).astype(jnp.bfloat16), 'tp')  14.5 us
    all_to_all x1, waiting for transfers between devices, on_device(): lax.all_to_all(expert_sum.reshape(sources, held_slots, -1), 'ep', split_a...  11.1 us
    all_to_all x1, waiting for transfers between devices, on_device(): lax.all_to_all(outgoing, 'ep', split_axis=0, concat_axis=0, tiled=True)  10.9 us
    all_to_all x1, waiting for transfers between devices, on_device(): lax.all_to_all(column_part, 'ep', split_axis=0, concat_axis=1, tiled=True)  7.44 us
  transfers between devices with their start and end apart: 6, of which 6 were waited for; matrix products, arithmetic and copies ran while one was open for 4% of the time, Pallas kernels for 0%

profile of v1, /device:TPU:0, one launch (start us, length us, event | category | flops | bytes accessed | tf_op | source)
XLA Modules:
  0.0 254.6 jit_solution(13918871230000059889)
XLA Ops:
  7.2 1.0 fusion.25
  8.3 0.9 fusion.27
  9.4 15.7 %all_to_all.34 = bf16[16,16,128]{2,1,0:T(8,128)(2,1)S(1)} all-to-all(bf16[16,16,128]{2,1,0:T(8,128)(2,1)S(1)} %constant_dynamic-update-slice_fusion), channel_id=1, replica_groups=mesh['ep'=16,'tp'=2] {'ep'}, dimensions={0} | all-to-all | bytes 131072 | tf_op jit(solution)/shard_map/all_to_all | solution.py:89
  25.1 2.8 %fusion.11 = f32[256,2048]{1,0:T(8,128)} fusion(bf16[256,128]{1,0:T(8,128)(2,1)S(1)} %bitcast.114, bf16[128,512]{1,0:T(8,128)(2,1)} %param.30, bf16[128,512]{1,0:T(8,128)(2,1)} %param.29, bf16[128,512]{1,0:T(8,128)(2,1)} %param.28, bf16[128,512]{1,0:T(8,128)(2,1)} %param.27), kind=kOutput, calls=%fused_computation.18 | convolution fusion | flops 136314880 | bytes 2686976 | tf_op jit(solution)/shard_map/dot_general | solution.py:93
  29.1 77.1 %reduce-scatter.2.cloned.1.call-done = f32[16,2048]{1,0:T(8,128)} async-done(((f32[256,2048]{1,0:T(8,128)}), f32[16,2048]{1,0:T(8,128)}) %reduce-scatter.2.cloned.1.call-update) | async-done | bytes 131088 | tf_op jit(solution)/shard_map/reduce_scatter | solution.py:92
  106.2 0.9 convert.9
  107.6 5.3 %fusion.61 = f32[16,8,1,64]{3,2,1,0:T(1,128)S(1)} fusion(f32[16,8,64,1]{2,3,1,0:T(1,128)S(1)} %bitcast.112, f32[16,8,64,64]{3,2,1,0:T(8,128)} %param.22), kind=kOutput, calls=%fused_computation.133 | convolution fusion | flops 6291456 | bytes 2162688 | tf_op jit(solution)/shard_map/shd,shde->she/dot_general | solution.py:46
  113.3 38.2 %all_gather.3 = bf16[256,512]{1,0:T(8,128)(2,1)S(1)} all-gather(bf16[16,512]{1,0:T(8,128)(2,1)S(1)} %fusion.45), channel_id=1, replica_groups=mesh['ep'=16,'tp'=2] {'ep'}, dimensions={0}, use_global_device_ids=true | all-gather | bytes 278528 | tf_op jit(solution)/shard_map/all_gather | solution.py:108
  152.3 3.5 %all-to-all-start.1 = ((bf16[16,16,128]{2,1,0:T(8,128)(2,1)}), bf16[16,16,128]{2,1,0:T(8,128)(2,1)S(1)}, u32[]{:S(2)}, u32[]{:S(2)}) async-start(bf16[16,16,128]{2,1,0:T(8,128)(2,1)} %bitcast.21), calls=%async_computation.2 | async-start | bytes 131072 | tf_op jit(solution)/shard_map/all_to_all | solution.py:112
  155.9 7.4 %all-to-all-done.1 = bf16[16,16,128]{2,1,0:T(8,128)(2,1)S(1)} async-done(((bf16[16,16,128]{2,1,0:T(8,128)(2,1)}), bf16[16,16,128]{2,1,0:T(8,128)(2,1)S(1)}, u32[]{:S(2)}, u32[]{:S(2)}) %all-to-all-start.1) | async-done | bytes 65568 | tf_op jit(solution)/shard_map/all_to_all | solution.py:112
  164.1 14.5 %all-reduce.4.cloned.1.call-done = bf16[16,2048]{1,0:T(8,128)(2,1)} async-done(((bf16[16,2048]{1,0:T(8,128)(2,1)}), bf16[16,2048]{1,0:T(8,128)(2,1)}) %all-reduce.4.cloned.1.call-update) | async-done | bytes 65552 | tf_op jit(solution)/shard_map/psum | solution.py:116
  178.6 1.0 fusion.23
  179.6 0.9 fusion.28
  180.6 1.1 fusion.1
  181.8 6.8 %all-to-all-start.2 = ((bf16[16,8,2048]{2,1,0:T(8,128)(2,1)}), bf16[16,8,2048]{2,1,0:T(8,128)(2,1)S(1)}, u32[]{:S(2)}, u32[]{:S(2)}) async-start(bf16[16,8,2048]{2,1,0:T(8,128)(2,1)} %fusion.1), calls=%async_computation.3 | async-start | bytes 1048576 | tf_op jit(solution)/shard_map/all_to_all | solution.py:145
  188.7 1.5 fusion.59
  190.2 3.0 %convolution_convert_fusion.2 = bf16[16,2048]{1,0:T(8,128)(2,1)} fusion(bf16[256,2048]{1,0:T(8,128)(2,1)} %param.39, bf16[2048,256]{1,0:T(8,128)(2,1)} %param.38, f32[16,256]{1,0:T(8,128)S(1)} %fusion.59, bf16[16,2048]{1,0:T(8,128)(2,1)S(1)} %fusion.28, f32[2048]{0:T(1024)S(1)} %copy-done.4, f32[16]{0:T(128)S(1)} %add_rsqrt_fusion.2), kind=kOutput, calls=%fused_computation.6 | convolution fusion | flops 33742848 | bytes 2252864 | tf_op jit(solution)/shard_map/dot_general | solution.py:164
  193.2 10.9 %all-to-all-done.2 = bf16[16,8,2048]{2,1,0:T(8,128)(2,1)S(1)} async-done(((bf16[16,8,2048]{2,1,0:T(8,128)(2,1)}), bf16[16,8,2048]{2,1,0:T(8,128)(2,1)S(1)}, u32[]{:S(2)}, u32[]{:S(2)}) %all-to-all-start.2) | async-done | bytes 524320 | tf_op jit(solution)/shard_map/all_to_all | solution.py:145
  204.1 1.5 fusion.9
  205.7 1.6 convolution_convert_fusion
  207.3 17.3 %all-reduce.6.cloned.1.call-done = (bf16[16,8,2048]{2,1,0:T(8,128)(2,1)}, bf16[16,2048]{1,0:T(8,128)(2,1)}) async-done(((bf16[16,8,2048]{2,1,0:T(8,128)(2,1)}, bf16[16,2048]{1,0:T(8,128)(2,1)}), (bf16[16,8,2048]{2,1,0:T(8,128)(2,1)}, bf16[16,2048]{1,0:T(8,128)(2,1)})) %all-reduce.6.cloned.1.call-update) | async-done | bytes 589840 | tf_op jit(solution)/shard_map/psum | solution.py:154
  224.5 6.8 %all-to-all-start.3 = ((bf16[16,8,2048]{2,1,0:T(8,128)(2,1)}), bf16[16,8,2048]{2,1,0:T(8,128)(2,1)S(1)}, u32[]{:S(2)}, u32[]{:S(2)}) async-start(bf16[16,8,2048]{2,1,0:T(8,128)(2,1)} %get-tuple-element.2), calls=%async_computation.4 | async-start | bytes 1048576 | tf_op jit(solution)/shard_map/all_to_all | solution.py:155
  231.5 4.3 %multiply_add_fusion = f32[16,8,64,64]{3,2,1,0:T(8,128)} fusion(f32[16,8,64,64]{3,2,1,0:T(8,128)} %param.22, f32[16,8,64]{2,1,0:T(8,128)S(1)} %reshape.194, f32[16,8,64]{2,1,0:T(8,128)S(1)} %get-tuple-element.20, f32[8]{0:T(128)S(1)} %dynamic_slice.3), kind=kLoop, calls=%fused_computation.1 | loop fusion | flops 1572864 | bytes 4259872 | tf_op jit(solution)/shard_map/add | solution.py:52
  235.8 11.1 %all-to-all-done.3 = bf16[16,8,2048]{2,1,0:T(8,128)(2,1)S(1)} async-done(((bf16[16,8,2048]{2,1,0:T(8,128)(2,1)}), bf16[16,8,2048]{2,1,0:T(8,128)(2,1)S(1)}, u32[]{:S(2)}, u32[]{:S(2)}) %all-to-all-start.3) | async-done | bytes 524320 | tf_op jit(solution)/shard_map/all_to_all | solution.py:155
  (79 shorter events, 5.2 us)
Async XLA Ops:
  7.2 198.5 %copy-start = (bf16[1,256,2048]{2,1,0:T(8,128)(2,1)S(1)}, bf16[1,256,2048]{2,1,0:T(8,128)(2,1)}, u32[]{:S(2)}) copy-start(bf16[1,256,2048]{2,1,0:T(8,128)(2,1)} %param.36) | copy-start | bytes 3145732
  7.2 20.8 %copy-start.10 = (s32[16]{0:T(128)S(1)}, s32[16]{0:T(128)}, u32[]{:S(2)}) copy-start(s32[16]{0:T(128)} %param.21) | copy-start | bytes 196
  7.2 20.9 %copy-start.6 = (s32[16,6]{0,1:T(8,128)S(1)}, s32[16,6]{0,1:T(8,128)}, u32[]{:S(2)}) copy-start(s32[16,6]{0,1:T(8,128)} %param.32) | copy-start | bytes 1156
  7.2 99.0 %reduce-scatter.2.cloned.1.call-start = ((), (), s32[]{:S(2)}) async-start(), calls=%async_computation.5 | async-start | bytes 2228224 | tf_op jit(solution)/shard_map/reduce_scatter | solution.py:92
  28.0 123.5 %copy-start.3 = (bf16[512,128]{1,0:T(8,128)(2,1)S(1)}, bf16[512,128]{1,0:T(8,128)(2,1)}, u32[]{:S(2)}) copy-start(bf16[512,128]{1,0:T(8,128)(2,1)} %param.31) | copy-start | bytes 393220
  28.0 151.6 %copy-start.2 = (bf16[16,2048]{1,0:T(8,128)(2,1)S(1)}, bf16[16,2048]{1,0:T(8,128)(2,1)}, u32[]{:S(2)}) copy-start(bf16[16,2048]{1,0:T(8,128)(2,1)} %param.20) | copy-start | bytes 196612
  28.0 151.6 %copy-start.7 = (f32[2048]{0:T(1024)S(1)}, f32[2048]{0:T(1024)}, u32[]{:S(2)}) copy-start(f32[2048]{0:T(1024)} %param.24) | copy-start | bytes 24580
  28.0 152.6 %copy-start.4 = (f32[2048]{0:T(1024)S(1)}, f32[2048]{0:T(1024)}, u32[]{:S(2)}) copy-start(f32[2048]{0:T(1024)} %param.25) | copy-start | bytes 24580
  113.2 92.5 %copy-start.1 = (bf16[1,2048,256]{2,1,0:T(8,128)(2,1)S(1)}, bf16[1,2048,256]{2,1,0:T(8,128)(2,1)}, u32[]{:S(2)}) copy-start(bf16[1,2048,256]{2,1,0:T(8,128)(2,1)} %param.35) | copy-start | bytes 3145732
  152.3 11.0 %all-to-all-start.1 = ((bf16[16,16,128]{2,1,0:T(8,128)(2,1)}), bf16[16,16,128]{2,1,0:T(8,128)(2,1)S(1)}, u32[]{:S(2)}, u32[]{:S(2)}) async-start(bf16[16,16,128]{2,1,0:T(8,128)(2,1)} %bitcast.21), calls=%async_computation.2 | async-start | bytes 131072 | tf_op jit(solution)/shard_map/all_to_all | solution.py:112
  155.8 22.7 %all-reduce.4.cloned.1.call-start = ((), (), s32[]{:S(2)}) async-start(), calls=%async_computation.6 | async-start | bytes 131072 | tf_op jit(solution)/shard_map/psum | solution.py:116
  181.8 22.3 %all-to-all-start.2 = ((bf16[16,8,2048]{2,1,0:T(8,128)(2,1)}), bf16[16,8,2048]{2,1,0:T(8,128)(2,1)S(1)}, u32[]{:S(2)}, u32[]{:S(2)}) async-start(bf16[16,8,2048]{2,1,0:T(8,128)(2,1)} %fusion.1), calls=%async_computation.3 | async-start | bytes 1048576 | tf_op jit(solution)/shard_map/all_to_all | solution.py:145
  188.6 35.9 %all-reduce.6.cloned.1.call-start = ((), (), s32[]{:S(2)}) async-start(), calls=%async_computation.7 | async-start | bytes 1179648 | tf_op jit(solution)/shard_map/psum | solution.py:154
  190.2 41.2 %copy-start.9 = (f32[16,6]{0,1:T(8,128)S(1)}, f32[16,6]{0,1:T(8,128)}, u32[]{:S(2)}) copy-start(f32[16,6]{0,1:T(8,128)} %param.33) | copy-start | bytes 1156
  224.5 22.3 %all-to-all-start.3 = ((bf16[16,8,2048]{2,1,0:T(8,128)(2,1)}), bf16[16,8,2048]{2,1,0:T(8,128)(2,1)S(1)}, u32[]{:S(2)}, u32[]{:S(2)}) async-start(bf16[16,8,2048]{2,1,0:T(8,128)(2,1)} %get-tuple-element.2), calls=%async_computation.4 | async-start | bytes 1048576 | tf_op jit(solution)/shard_map/all_to_all | solution.py:155
  231.5 15.4 %copy-start.5 = (bf16[16,2048]{1,0:T(8,128)(2,1)S(1)}, bf16[16,2048]{1,0:T(8,128)(2,1)}, u32[]{:S(2)}) copy-start(bf16[16,2048]{1,0:T(8,128)(2,1)} %get-tuple-element.3) | copy-start | bytes 196612
  231.5 15.8 %copy-start.8 = (f32[2048]{0:T(1024)S(1)}, f32[2048]{0:T(1024)}, u32[]{:S(2)}) copy-start(f32[2048]{0:T(1024)} %param.26) | copy-start | bytes 24580
Sparse Core Ops, SparseCore 0:
  28.1 78.0 reduce-scatter.1
  164.1 14.3 all-reduce.3
  207.4 17.0 all-reduce.5
